TPU v7x, 32 devices: a whole 2x2x4 slice. The times are simulated.
32 devices in a mesh: fs: 8 (over z, x), tp: 4 (over y, core).
Axes of the slice: x: 2, y: 2, z: 4, core: 2. Of those that a mesh axis runs over, the one named last changes fastest.
Arguments:
- tokens: bfloat16 [4096, 2048], P('fs', 'tp'), may hold values from -6 to 6
- pre_gain: float32 [2048], P('fs'), may hold values from 0.1 to 1.9
- gate_weight: float32 [2048, 6144], P('fs', 'tp'), may hold values from -0.125 to 0.125
- up_weight: float32 [2048, 6144], P('fs', 'tp'), may hold values from -0.125 to 0.125
- down_weight: float32 [2048, 6144], P('fs', 'tp'), may hold values from -0.078125 to 0.078125
- post_gain: float32 [2048], P('tp'), may hold values from 0.1 to 1.9
Outputs:
- result: bfloat16 [4096, 2048], P('fs', 'tp')
- gate_ready: bfloat16 [2048, 6144], P(None, 'tp')
- up_ready: bfloat16 [2048, 6144], P(None, 'tp')
- down_ready: bfloat16 [2048, 6144], P(None, 'tp')
All inputs are finite; a program needn't handle non-finite values.
Results may differ from a plain program's by a relative error of at most 0.015.
Values may be sent and summed in bfloat16 or wider, within the bound.
A program may use at most 128 MiB of HBM per device.

v0:
```python
import jax
import jax.numpy as jnp
from jax import lax
from jax.sharding import PartitionSpec as P

EPS = 1e-06


def shards(tokens, pre_gain, gate_weight, up_weight, down_weight, post_gain):
    gate_local = (pre_gain[:, None] * gate_weight).astype(jnp.bfloat16)
    up_local = (pre_gain[:, None] * up_weight).astype(jnp.bfloat16)
    down_local = down_weight.astype(jnp.bfloat16)
    whole = lax.all_gather(tokens, "tp", axis=1, tiled=True)
    widened = whole.astype(jnp.float32)
    width = whole.shape[1]
    normalized = (
        widened * lax.rsqrt(jnp.mean(widened * widened, axis=1, keepdims=True) + EPS)
    ).astype(jnp.bfloat16)
    contract = (((1,), (1,)), ((), ()))
    gate_full, up_full, down_full = (
        lax.all_gather(gate_local, "fs", axis=0, tiled=True),
        lax.all_gather(up_local, "fs", axis=0, tiled=True),
        lax.all_gather(down_local, "fs", axis=0, tiled=True),
    )
    gate = jnp.dot(normalized, gate_full, preferred_element_type=jnp.float32)
    up = jnp.dot(normalized, up_full, preferred_element_type=jnp.float32)
    hidden = (jax.nn.silu(gate) * up).astype(jnp.bfloat16)
    partial_value = lax.dot_general(hidden, down_full, contract, preferred_element_type=jnp.float32)
    share = lax.psum_scatter(
        partial_value.astype(jnp.bfloat16), "tp", scatter_dimension=1, tiled=True
    ).astype(jnp.float32)
    squares = lax.psum(jnp.sum(share * share, axis=1, keepdims=True), "tp")
    scaling = lax.rsqrt(squares / width + EPS)
    result = (share * scaling * post_gain[None, :]).astype(jnp.bfloat16)
    return (result, gate_full, up_full, down_full)


def solution(mesh):
    return jax.shard_map(
        shards,
        mesh=mesh,
        in_specs=(P("fs", "tp"), P("fs"), P("fs", "tp"), P("fs", "tp"), P("fs", "tp"), P("tp")),
        out_specs=(P("fs", "tp"), P(None, "tp"), P(None, "tp"), P(None, "tp")),
        check_vma=False,
    )
```

profile of v0, /device:TPU:0, one launch (start us, length us, event | category | flops | bytes accessed | tf_op | source)
XLA Modules:
  0.0 406.3 jit_solution(389480162345285521)
XLA Ops:
  7.2 0.0 all-gather.5.cloned.1.call-start
  7.2 0.7 all-gather.5.cloned.1.call-update
  7.9 0.0 copy-start.1
  7.9 0.0 all-gather.7.cloned.1.call-start
  8.0 3.5 multiply_convert_fusion.1
  11.5 0.0 all-gather.7.cloned.1.call-update
  11.5 0.0 all-gather.9.cloned.1.call-start
  11.6 0.7 all-gather.9.cloned.1.call-update
  12.3 0.0 all-gather.11.cloned.1.call-start
  12.3 0.0 copy-done.1
  12.3 1.0 convert_element_type.32
  13.3 0.0 all-gather.11.cloned.1.call-update
  13.3 0.0 reduce-scatter.2.cloned.1.call-start
  13.4 21.5 %all-gather.5.cloned.1.call-done = bf16[512,2048]{1,0:T(8,128)(2,1)} async-done(((bf16[512,512]{1,0:T(8,128)(2,1)}), bf16[512,2048]{1,0:T(8,128)(2,1)}) %all-gather.5.cloned.1.call-update) | async-done | bytes 2097168 | tf_op jit(solution)/shard_map/all_gather | solution.py:13
  34.9 2.1 fusion
  36.9 0.0 copy-start
  37.0 99.4 %all-gather.7.cloned.1.call-done = bf16[2048,1536]{1,0:T(8,128)(2,1)} async-done(((bf16[256,1536]{1,0:T(8,128)(2,1)}), bf16[2048,1536]{1,0:T(8,128)(2,1)}) %all-gather.7.cloned.1.call-update) | async-done | bytes 6291472 | tf_op jit(solution)/shard_map/all_gather | solution.py:21
  136.3 8.5 %fusion.7 = f32[512,1536]{1,0:T(8,128)} fusion(bf16[2048,1536]{1,0:T(8,128)(2,1)} %all-gather.7.cloned.1.call-done, bf16[512,2048]{1,0:T(8,128)(2,1)} %all-gather.5.cloned.1.call-done, f32[512]{0:T(512)S(1)} %add_rsqrt_fusion.1), kind=kOutput, calls=%fused_computation.14 | convolution fusion | flops 3224371200 | bytes 11536384 | tf_op jit(solution)/shard_map/dot_general | solution.py:25
  144.9 0.0 copy-start.2
  144.9 91.1 %all-gather.9.cloned.1.call-done = bf16[2048,1536]{1,0:T(8,128)(2,1)} async-done(((bf16[256,1536]{1,0:T(8,128)(2,1)}), bf16[2048,1536]{1,0:T(8,128)(2,1)}) %all-gather.9.cloned.1.call-update) | async-done | bytes 6291472 | tf_op jit(solution)/shard_map/all_gather | solution.py:22
  236.0 99.5 %all-gather.11.cloned.1.call-done = bf16[2048,1536]{1,0:T(8,128)(2,1)} async-done(((bf16[256,1536]{1,0:T(8,128)(2,1)}), bf16[2048,1536]{1,0:T(8,128)(2,1)}) %all-gather.11.cloned.1.call-update) | async-done | bytes 6291472 | tf_op jit(solution)/shard_map/all_gather | solution.py:23
  335.5 0.0 copy-done
  335.5 13.6 %convolution_convert_fusion = bf16[512,2048]{1,0:T(8,128)(2,1)} fusion(bf16[2048,1536]{1,0:T(8,128)(2,1)} %all-gather.11.cloned.1.call-done, bf16[2048,1536]{1,0:T(8,128)(2,1)} %all-gather.9.cloned.1.call-done, f32[512,1536]{1,0:T(8,128)} %fusion.7, bf16[512,2048]{1,0:T(8,128)(2,1)S(1)} %copy-done, f32[512]{0:T(512)S(1)} %add_rsqrt_fusion.1), kind=kOutput, calls=%fused_computation.6 | convolution fusion | flops 6451363840 | bytes 19924992 | tf_op jit(solution)/shard_map/dot_general | solution.py:28
  349.2 0.0 reduce-scatter.2.cloned.1.call-update
  349.2 29.5 %reduce-scatter.2.cloned.1.call-done = bf16[512,512]{1,0:T(8,128)(2,1)} async-done(((bf16[512,2048]{1,0:T(8,128)(2,1)}), bf16[512,512]{1,0:T(8,128)(2,1)}) %reduce-scatter.2.cloned.1.call-update) | async-done | bytes 524304 | tf_op jit(solution)/shard_map/reduce_scatter | solution.py:29
  378.7 1.2 fusion.3
  379.9 5.8 %psum.7 = f32[512,1]{0,1:T(1,128)S(1)} all-reduce(f32[512,1]{0,1:T(1,128)S(1)} %bitcast.10), channel_id=1, replica_groups=mesh['fs'=8,'tp'=4] {'tp'}, use_global_device_ids=true, to_apply=%region_3.4 | all-reduce | flops 512 | bytes 4096 | tf_op jit(solution)/shard_map/psum | solution.py:32
  385.7 0.0 copy-done.2
  385.7 0.0 slice-start
  385.7 2.2 fusion.5
  387.8 0.0 slice-start.1
  387.8 0.0 slice-start.2
  387.8 6.1 %copy.13 = bf16[2048,1536]{1,0:T(8,128)(2,1)} copy(bf16[2048,1536]{1,0:T(8,128)(2,1)} %all-gather.7.cloned.1.call-done) | data formatting | bytes 12582912
  393.9 0.0 slice-done
  393.9 0.0 slice-done.1
  393.9 0.0 slice-start.3
  393.9 2.8 copy.14
  396.8 0.0 slice-done.2
  396.8 0.3 slice-done.3
  397.0 2.7 copy.15
  (4 shorter events, 0.0 us)
Async XLA Ops:
  7.2 27.7 %all-gather.5.cloned.1.call-start = ((), (), s32[]{:S(2)}) async-start(), calls=%async_computation.1 | async-start | bytes 2621440 | tf_op jit(solution)/shard_map/all_gather | solution.py:13
  7.9 4.4 %copy-start.1 = (f32[256,1536]{1,0:T(8,128)S(1)}, f32[256,1536]{1,0:T(8,128)}, u32[]{:S(2)}) copy-start(f32[256,1536]{1,0:T(8,128)} %param.10) | copy-start | bytes 4718596
  7.9 128.4 %all-gather.7.cloned.1.call-start = ((), (), s32[]{:S(2)}) async-start(), calls=%async_computation.2 | async-start | bytes 7077888 | tf_op jit(solution)/shard_map/all_gather | solution.py:21
  11.5 224.5 %all-gather.9.cloned.1.call-start = ((), (), s32[]{:S(2)}) async-start(), calls=%async_computation.3 | async-start | bytes 7077888 | tf_op jit(solution)/shard_map/all_gather | solution.py:22
  12.3 323.3 %all-gather.11.cloned.1.call-start = ((), (), s32[]{:S(2)}) async-start(), calls=%async_computation.4 | async-start | bytes 7077888 | tf_op jit(solution)/shard_map/all_gather | solution.py:23
  13.3 365.4 %reduce-scatter.2.cloned.1.call-start = ((), (), s32[]{:S(2)}) async-start(), calls=%async_computation.5 | async-start | bytes 2621440 | tf_op jit(solution)/shard_map/reduce_scatter | solution.py:29
  36.9 298.6 %copy-start = (bf16[512,2048]{1,0:T(8,128)(2,1)S(1)}, bf16[512,2048]{1,0:T(8,128)(2,1)}, u32[]{:S(2)}) copy-start(bf16[512,2048]{1,0:T(8,128)(2,1)} %all-gather.5.cloned.1.call-done) | copy-start | bytes 6291460
  144.9 240.8 %copy-start.2 = (f32[512]{0:T(512)S(1)}, f32[512]{0:T(512)}, u32[]{:S(2)}) copy-start(f32[512]{0:T(512)} %param.11) | copy-start | bytes 6148
  385.7 8.2 %slice-start = ((s8[6291456]{0:T(1024)(128)(4,1)}), s8[4194304]{0:T(1024)(128)(4,1)S(1)}, s32[]{:S(2)}) async-start(s8[6291456]{0:T(1024)(128)(4,1)} %bitcast.5), calls=%async_computation.6 | async-start | bytes 8388608
  387.8 6.1 %slice-start.1 = ((s8[6291456]{0:T(1024)(128)(4,1)}), s8[2097152]{0:T(1024)(128)(4,1)S(1)}, s32[]{:S(2)}) async-start(s8[6291456]{0:T(1024)(128)(4,1)} %bitcast.5), calls=%async_computation.7 | async-start | bytes 4194304
  387.8 8.9 %slice-start.2 = ((s8[6291456]{0:T(1024)(128)(4,1)}), s8[4194304]{0:T(1024)(128)(4,1)S(1)}, s32[]{:S(2)}) async-start(s8[6291456]{0:T(1024)(128)(4,1)} %bitcast.7), calls=%async_computation.8 | async-start | bytes 8388608
  393.9 3.1 slice-start.3
Sparse Core Ops, SparseCore 0:
  9.5 25.2 all-gather.4
  37.6 98.6 all-gather.6
  139.1 96.8 all-gather.8
  238.6 96.8 all-gather.10
  349.3 29.3 reduce-scatter.1
where the time goes:
time: 407 us; the launch traced here: 406 us
  waiting for transfers between devices  342 us (84%)
  matrix products  22.2 us (5%)
  between operations  13.8 us (3%)
  local copies, waits for them, and re-layouts  11.9 us (3%)
  other arithmetic  9.99 us (2%)
  blocking collectives  5.76 us (1%)
    all_gather x1, waiting for transfers between devices, shards(): lax.all_gather(down_local, 'fs', axis=0, tiled=True)  99.5 us
    all_gather x1, waiting for transfers between devices, shards(): lax.all_gather(gate_local, 'fs', axis=0, tiled=True)  99.4 us
    all_gather x1, waiting for transfers between devices, shards(): lax.all_gather(up_local, 'fs', axis=0, tiled=True)  91.1 us
    reduce_scatter x1, waiting for transfers between devices, shards(): lax.psum_scatter(partial_value.astype(jnp.bfloat16), 'tp', scatter_dimens...  29.5 us
    all_gather x1, waiting for transfers between devices, shards(): whole = lax.all_gather(tokens, 'tp', axis=1, tiled=True)  21.5 us
    dot_general x1, matrix products, shards(): lax.dot_general(hidden, down_full, contract, preferred_element_type=jnp.f...  13.6 us
    unnamed x17, local copies, waits for them, and re-layouts  11.9 us
    dot_general x1, matrix products, shards(): gate = jnp.dot(normalized, gate_full, preferred_element_type=jnp.float32)  8.54 us
  transfers between devices with their start and end apart: 5, of which 5 were waited for; matrix products, arithmetic and copies ran while one was open for 4% of the time, Pallas kernels for 0%

commit v1 on v0

v1 whole, which is shorter than its diff:
```python
import functools

import jax
import jax.numpy as jnp
from jax import lax
from jax.experimental import pallas as pl
from jax.experimental.pallas import tpu as pltpu
from jax.sharding import PartitionSpec as P

EPS = 1e-06
MESH = pl.DeviceIdType.MESH
Q_PART, P_PART = 0, 1
UP, DOWN, RIGHT, LEFT = 0, 1, 2, 3


def split_rows(depth, lines, cols):
    if cols == 1 or lines == 1:
        return [0, 0, 0]
    share = ((cols - 1) * lines - (lines - 1)) / (2 * (lines - 1) * (cols - 1))
    share = min(max(share, 0.0), 1.0)
    units = min(int(round(3 * depth * share / 16)), 3 * (depth // 16))
    return [16 * (units // 3 + (1 if m >= 3 - units % 3 else 0)) for m in range(3)]


def kernel(
    fs, tp, lines, cols, first_rows,
    tokens, gate_own, up_own, down_own, post_gain,
    result, gate_out, up_out, down_out,
    held, whole, normed, gate, hidden, part, parts_in, squares, squares_in,
    send_sem, recv_sem, own_sem, out_sem, tok_send, tok_recv, tok_own,
    rs_send, rs_recv, sq_send, sq_recv,
):
    owns, outs = (gate_own, up_own, down_own), (gate_out, up_out, down_out)
    depth, width = gate_own.shape
    rows, block = tokens.shape
    me_fs, me = lax.axis_index("fs"), lax.axis_index("tp")
    z, x = me_fs // cols, lax.rem(me_fs, cols)
    finals = []

    sides = {
        UP: (z < lines - 1, me_fs + cols),
        DOWN: (z > 0, me_fs - cols),
        RIGHT: (x < cols - 1, me_fs + 1),
        LEFT: (x > 0, me_fs - 1),
    }
    peers = [lax.rem(me + j, tp) for j in range(1, tp)]

    def piece(m, which, shard):
        start, size = (0, first_rows[m]) if which == P_PART else (first_rows[m], depth - first_rows[m])
        return held.at[m, pl.ds(pl.multiple_of(shard * depth + start, 16), size), :]

    def describe(m, which, shard, side, target):
        ref = piece(m, which, shard)
        return pltpu.make_async_remote_copy(
            src_ref=ref, dst_ref=ref,
            send_sem=send_sem.at[m, which, shard, side],
            recv_sem=recv_sem.at[m, which, shard],
            device_id={"fs": target, "tp": me}, device_id_type=MESH,
        )

    def empty(m, which):
        return (first_rows[m] if which == P_PART else depth - first_rows[m]) == 0

    def send(m, which, shard, side, extra=None):
        if empty(m, which):
            return
        there, target = sides[side]
        cond = there if extra is None else jnp.logical_and(there, extra)

        @pl.when(cond)
        def _():
            describe(m, which, shard, side, target).start()

        def finish():
            @pl.when(cond)
            def _():
                describe(m, which, shard, side, target).wait_send()

        finals.append(finish)

    def arrive(m, which, shard, cond):
        if empty(m, which):
            return

        @pl.when(cond)
        def _():
            describe(m, which, shard, 0, lax.rem(me_fs + 1, fs)).wait_recv()

    barrier = pltpu.get_barrier_semaphore()
    for side in sides:
        there, target = sides[side]

        @pl.when(there)
        def _():
            pl.semaphore_signal(barrier, inc=1, device_id={"fs": target, "tp": me}, device_id_type=MESH)

    for peer in peers:
        pl.semaphore_signal(barrier, inc=1, device_id={"fs": me_fs, "tp": peer}, device_id_type=MESH)

    own_copies = [pltpu.make_async_copy(owns[m], held.at[m, pl.ds(pl.multiple_of(me_fs * depth, 16), depth), :], own_sem.at[m]) for m in range(3)]
    for c in own_copies:
        c.start()
    own_tokens = pltpu.make_async_copy(tokens, whole.at[me], tok_own)
    own_tokens.start()
    pl.semaphore_wait(barrier, tp - 1 + sum(there.astype(jnp.int32) for there, _ in sides.values()))

    def token_copy(j):
        return pltpu.make_async_remote_copy(
            src_ref=tokens, dst_ref=whole.at[me], send_sem=tok_send.at[j], recv_sem=tok_recv.at[j],
            device_id={"fs": me_fs, "tp": peers[j]}, device_id_type=MESH,
        )

    def start_own(m):
        own_copies[m].wait()
        for which in (P_PART, Q_PART):
            for side in (RIGHT, LEFT):
                send(m, which, me_fs, side)
            if which == Q_PART:
                for side in (UP, DOWN):
                    send(m, which, me_fs, side)

    start_own(0)
    for j in range(tp - 1):
        token_copy(j).start()

    def normalize():
        own_tokens.wait()
        for j in range(tp - 1):
            token_copy(j).wait_recv()
        step = 64

        @pl.loop(0, rows // step)
        def _(i):
            here = pl.ds(pl.multiple_of(i * step, step), step)
            total = jnp.zeros((step, 1), jnp.float32)
            for t in range(tp):
                v = whole[t, here, :].astype(jnp.float32)
                total = total + jnp.sum(v * v, axis=1, keepdims=True)
            scale = lax.rsqrt(total / (tp * block) + EPS)
            for t in range(tp):
                v = whole[t, here, :].astype(jnp.float32)
                normed[here, t * block:(t + 1) * block] = (v * scale).astype(jnp.bfloat16)

    def along_x(m, which, line, cond=None):
        for r in range(cols - 1):
            for side, column in ((RIGHT, x - 1 - r), (LEFT, x + 1 + r)):
                there = jnp.logical_and(column >= 0, column < cols)
                if cond is not None:
                    there = jnp.logical_and(there, cond)
                arrive(m, which, line * cols + column, there)
                if r < cols - 2:
                    send(m, which, line * cols + column, side, there)

    def along_z(m, which, s, columns):
        for side, line in ((UP, z - 1 - s), (DOWN, z + 1 + s)):
            there = jnp.logical_and(line >= 0, line < lines)
            for column in columns:
                shard = line * cols + column
                arrive(m, which, shard, there)
                if s < lines - 2:
                    send(m, which, shard, side, there)
                if which == Q_PART:
                    send(m, which, shard, RIGHT, there)
                    send(m, which, shard, LEFT, there)

    def first_half(m):
        for s in range(lines - 1):
            along_z(m, Q_PART, s, [x])
        along_x(m, P_PART, z)
        for column in range(cols):
            for side in (UP, DOWN):
                send(m, P_PART, z * cols + column, side)

    def whole_out(m):
        return pltpu.make_async_copy(held.at[m], outs[m], out_sem.at[m])

    tile = 256
    for m in range(2):
        first_half(m)
        for s in range(lines - 1):
            along_z(m, P_PART, s, range(cols))
        start_own(m + 1)
        if m == 0:
            normalize()
        along_x(m, Q_PART, z)
        for s in range(lines - 1):
            for line in (z - 1 - s, z + 1 + s):
                along_x(m, Q_PART, line, jnp.logical_and(line >= 0, line < lines))
        whole_out(m).start()

        @pl.loop(0, width // tile)
        def _(i):
            here = pl.ds(pl.multiple_of(i * tile, tile), tile)
            product = jnp.dot(normed[...], held[m, :, here], preferred_element_type=jnp.float32)
            if m == 0:
                gate[:, here] = product
            else:
                g = gate[:, here]
                hidden[:, here] = (g / (1.0 + jnp.exp(-g)) * product).astype(jnp.bfloat16)

    def share_copy(line, slot, sem_index):
        return pltpu.make_async_remote_copy(
            src_ref=part.at[line], dst_ref=parts_in.at[slot], send_sem=rs_send.at[line], recv_sem=rs_recv.at[sem_index],
            device_id={"fs": me_fs, "tp": line}, device_id_type=MESH,
        )

    group = cols * depth

    def group_out(line):
        here = pl.ds(pl.multiple_of(line * group, group), group)
        return pltpu.make_async_copy(held.at[2, here, :], outs[2].at[here, :], out_sem.at[2 + line])

    def mix(line, cond):
        @pl.when(cond)
        def _():
            group_out(line).start()

            @pl.loop(0, group // tile)
            def _(i):
                here = pl.ds(pl.multiple_of(line * group + i * tile, tile), tile)
                product = lax.dot_general(
                    hidden[...], held[2, here, :], (((1,), (1,)), ((), ())), preferred_element_type=jnp.float32
                )
                part[line, :, pl.ds(pl.multiple_of(i * tile, tile), tile)] = product.astype(jnp.bfloat16)

            @pl.when(line != me)
            def _():
                share_copy(line, me, me).start()

    first_half(2)
    along_x(2, Q_PART, z)
    mix(z, z >= 0)
    for s in range(lines - 1):
        along_z(2, P_PART, s, range(cols))
        for line in (z - 1 - s, z + 1 + s):
            there = jnp.logical_and(line >= 0, line < lines)
            along_x(2, Q_PART, line, there)
            mix(line, there)

    for peer in peers:
        share_copy(peer, peer, peer).wait_recv()
    step = 128

    @pl.loop(0, rows // step)
    def _(i):
        here = pl.ds(pl.multiple_of(i * step, step), step)
        total = part[me, here, :].astype(jnp.float32)
        for peer in peers:
            total = total + parts_in[peer, here, :].astype(jnp.float32)
        gate[here, 0:block] = total
        line = jnp.broadcast_to(jnp.sum(total * total, axis=1, keepdims=True), (step, 128))
        squares[:, here] = jnp.transpose(line)[0:8, :]

    def square_copy(j):
        return pltpu.make_async_remote_copy(
            src_ref=squares, dst_ref=squares_in.at[j], send_sem=sq_send.at[j], recv_sem=sq_recv.at[j],
            device_id={"fs": me_fs, "tp": peers[j]}, device_id_type=MESH,
        )

    for j in range(tp - 1):
        square_copy(j).start()
    for j in range(tp - 1):
        square_copy(j).wait_recv()
    gains = post_gain[0:1, :]

    @pl.loop(0, rows // step)
    def _(i):
        here = pl.ds(pl.multiple_of(i * step, step), step)
        total = squares[:, here]
        for j in range(tp - 1):
            total = total + squares_in[j, :, here]
        total = jnp.broadcast_to(total[0:1, :], (128, step))
        scale = lax.rsqrt(jnp.transpose(total)[:, 0:1] / (tp * block) + EPS)
        result[here, :] = (gate[here, 0:block] * scale * gains).astype(jnp.bfloat16)

    for finish in finals:
        finish()
    for j in range(tp - 1):
        token_copy(j).wait_send()
        square_copy(j).wait_send()
        share_copy(peers[j], me, me).wait_send()
    for m in range(2):
        whole_out(m).wait()
    for line in range(lines):
        group_out(line).wait()


def solution(mesh):
    fs, tp = mesh.shape["fs"], mesh.shape["tp"]
    lines, cols = tp, fs // tp

    def shards(tokens, pre_gain, gate_weight, up_weight, down_weight, post_gain):
        depth, width = gate_weight.shape
        rows, block = tokens.shape
        gate_own = (pre_gain[:, None] * gate_weight).astype(jnp.bfloat16)
        up_own = (pre_gain[:, None] * up_weight).astype(jnp.bfloat16)
        down_own = down_weight.astype(jnp.bfloat16)
        first_rows = split_rows(depth, lines, cols)
        any_space = pl.BlockSpec(memory_space=pl.ANY)
        vmem = pl.BlockSpec(memory_space=pltpu.VMEM)
        dma = pltpu.SemaphoreType.DMA
        ready = jax.ShapeDtypeStruct((fs * depth, width), jnp.bfloat16)
        return pl.pallas_call(
            functools.partial(kernel, fs, tp, lines, cols, first_rows),
            out_shape=(jax.ShapeDtypeStruct((rows, block), jnp.bfloat16), ready, ready, ready),
            in_specs=[any_space] * 4 + [vmem],
            out_specs=(vmem, any_space, any_space, any_space),
            scratch_shapes=[
                pltpu.VMEM((3, fs * depth, width), jnp.bfloat16),
                pltpu.VMEM((tp, rows, block), jnp.bfloat16),
                pltpu.VMEM((rows, tp * block), jnp.bfloat16),
                pltpu.VMEM((rows, max(width, block)), jnp.float32),
                pltpu.VMEM((rows, width), jnp.bfloat16),
                pltpu.VMEM((tp, rows, block), jnp.bfloat16),
                pltpu.VMEM((tp, rows, block), jnp.bfloat16),
                pltpu.VMEM((8, rows), jnp.float32),
                pltpu.VMEM((tp - 1, 8, rows), jnp.float32),
                dma((3, 2, fs, 4)), dma((3, 2, fs)), dma((3,)), dma((2 + lines,)),
                dma((tp - 1,)), dma((tp - 1,)), dma,
                dma((tp,)), dma((tp,)), dma((tp - 1,)), dma((tp - 1,)),
            ],
            compiler_params=pltpu.CompilerParams(collective_id=0, has_side_effects=True, vmem_limit_bytes=60 * 1024 * 1024),
        )(tokens, gate_own, up_own, down_own, post_gain[None, :])

    return jax.shard_map(
        shards,
        mesh=mesh,
        in_specs=(P("fs", "tp"), P("fs"), P("fs", "tp"), P("fs", "tp"), P("fs", "tp"), P("tp")),
        out_specs=(P("fs", "tp"), P(None, "tp"), P(None, "tp"), P(None, "tp")),
        check_vma=False,
    )
```

time: 407 us -> 230 us (0.57)
  waiting for transfers between devices: 342 us -> 0 us
  Pallas kernels: 0 us -> 208 us
  matrix products: 22.2 us -> 0 us
  between operations: 13.8 us -> 0.66 us
  blocking collectives: 5.76 us -> 0 us
  other arithmetic: 9.99 us -> 5.45 us
    all_gather x4 -> x0, waiting for transfers between devices: 312 us -> none  [the longest x1 99.5 us: shards(): lax.all_gather(down_local, 'fs', axis=0, tiled=True)]
    pallas_call x0 -> x1, Pallas kernels: none -> 208 us  [shards(): pl.pallas_call(functools.partial(kernel, fs, tp, lines, cols, first_rows)...]
    reduce_scatter x1 -> x0, waiting for transfers between devices: 29.5 us -> none  [shards(): lax.psum_scatter(partial_value.astype(jnp.bfloat16), 'tp', scatter_dimens...]
    dot_general x2 -> x0, matrix products: 22.2 us -> none  [the longest x1 13.6 us: shards(): lax.dot_general(hidden, down_full, contract, preferred_element_type=jnp.f...]
    psum x1 -> x0, blocking collectives: 5.76 us -> none  [shards(): squares = lax.psum(jnp.sum(share * share, axis=1, keepdims=True), 'tp')]
    unnamed x17 -> x14, local copies, waits for them, and re-layouts: 11.9 us -> 15.7 us
  transfers between devices with their start and end apart: 5 -> 0, of which waited for: 5 -> 0; matrix products, arithmetic and copies ran while one was open for 4% -> 0% of each run, Pallas kernels for 0% -> 0%
where the time goes in v1:
time: 230 us; the launch traced here: 229 us
  Pallas kernels  208 us (90%)
  local copies, waits for them, and re-layouts  15.7 us (7%)
  other arithmetic  5.45 us (2%)
    pallas_call x1, Pallas kernels, shards(): pl.pallas_call(functools.partial(kernel, fs, tp, lines, cols, first_rows)...  208 us
    unnamed x14, local copies, waits for them, and re-layouts  15.7 us

profile of v1, /device:TPU:0, one launch (start us, length us, event | category | flops | bytes accessed | tf_op | source)
XLA Modules:
  0.0 229.3 jit_solution(4490755308726683428)
XLA Ops:
  0.6 0.0 copy-start.1
  0.6 0.0 copy-start.2
  0.7 2.5 %convert_element_type.11.down_own = bf16[256,1536]{1,0:T(8,128)(2,1)} convert(f32[256,1536]{1,0:T(8,128)} %param.10) | non-fusion elementwise | flops 393216 | bytes 2359296 | tf_op jit(solution)/shard_map/convert_element_type | solution.py:297
  3.1 0.0 copy-done.1
  3.1 0.0 copy-done.2
  3.1 3.0 %multiply_convert_fusion = (bf16[256,1536]{1,0:T(8,128)(2,1)}, bf16[256,1536]{1,0:T(8,128)(2,1)}) fusion(f32[256,1536]{1,0:T(8,128)S(1)} %copy-done.1, f32[256]{0:T(256)S(1)} %copy-done.2, f32[256,1536]{1,0:T(8,128)} %param.8), kind=kLoop, calls=%fused_computation | loop fusion | flops 1572864 | bytes 4719616 | tf_op jit(solution)/shard_map/convert_element_type | solution.py:296
  6.1 207.5 %shard_map.93 = (bf16[512,512]{1,0:T(8,128)(2,1)}, bf16[2048,1536]{1,0:T(8,128)(2,1)}, bf16[2048,1536]{1,0:T(8,128)(2,1)}, bf16[2048,1536]{1,0:T(8,128)(2,1)}) custom-call(bf16[512,512]{1,0:T(8,128)(2,1)} %tokens.1, bf16[256,1536]{1,0:T(8,128)(2,1)} %get-tuple-element.5.gate_own, bf16[256,1536]{1,0:T(8,128)(2,1)} %get-tuple-element.4.up_own, ...), custom_call_target="tpu_custom_call" | custom-call | tf_op jit(solution)/shard_map/pallas_call | solution.py:303
  213.6 1.9 copy.14
  215.5 0.0 copy-start
  215.5 0.0 slice-start
  215.5 6.5 %copy.15 = bf16[2048,1536]{1,0:T(8,128)(2,1)} copy(bf16[2048,1536]{1,0:T(8,128)(2,1)} %get-tuple-element.11) | data formatting | bytes 12582912
  222.1 0.0 copy-done
  222.1 0.0 slice-start.1
  222.1 3.2 %copy.16 = bf16[2048,1536]{1,0:T(8,128)(2,1)} copy(bf16[2048,1536]{1,0:T(8,128)(2,1)S(1)} %copy-done) | data formatting | bytes 12582912
  225.3 0.0 slice-done
  225.3 1.4 slice-done.1
  226.6 2.7 %copy.17 = bf16[2048,1536]{1,0:T(8,128)(2,1)} copy(bf16[2048,1536]{1,0:T(8,128)(2,1)S(1)} %bitcast.2) | data formatting | bytes 12582912
  (1 shorter events, 0.0 us)
Async XLA Ops:
  0.6 2.5 %copy-start.1 = (f32[256,1536]{1,0:T(8,128)S(1)}, f32[256,1536]{1,0:T(8,128)}, u32[]{:S(2)}) copy-start(f32[256,1536]{1,0:T(8,128)} %param.9) | copy-start | bytes 4718596
  0.6 2.5 %copy-start.2 = (f32[256]{0:T(256)S(1)}, f32[256]{0:T(256)}, u32[]{:S(2)}) copy-start(f32[256]{0:T(256)} %param.7) | copy-start | bytes 3076
  215.5 6.6 %copy-start = (bf16[2048,1536]{1,0:T(8,128)(2,1)S(1)}, bf16[2048,1536]{1,0:T(8,128)(2,1)}, u32[]{:S(2)}) copy-start(bf16[2048,1536]{1,0:T(8,128)(2,1)} %get-tuple-element.12) | copy-start | bytes 18874372
  215.5 9.8 %slice-start = ((s8[6291456]{0:T(1024)(128)(4,1)}), s8[4194304]{0:T(1024)(128)(4,1)S(1)}, s32[]{:S(2)}) async-start(s8[6291456]{0:T(1024)(128)(4,1)} %bitcast.1), calls=%async_computation | async-start | bytes 8388608
  222.1 4.6 %slice-start.1 = ((s8[6291456]{0:T(1024)(128)(4,1)}), s8[2097152]{0:T(1024)(128)(4,1)S(1)}, s32[]{:S(2)}) async-start(s8[6291456]{0:T(1024)(128)(4,1)} %bitcast.1), calls=%async_computation.1 | async-start | bytes 4194304

commit v2 on v1

v2 whole, which is shorter than its diff:
```python
import functools

import jax
import jax.numpy as jnp
from jax import lax
from jax.experimental import pallas as pl
from jax.experimental.pallas import tpu as pltpu
from jax.sharding import PartitionSpec as P

EPS = 1e-06
MESH = pl.DeviceIdType.MESH
P_PART, Q_PART = 0, 1
UP, DOWN, RIGHT, LEFT = 0, 1, 2, 3


def kernel(
    fs, tp, lines, cols,
    tokens, pre_gain, gate_weight, up_weight, down_weight, post_gain,
    result, gate_out, up_out, down_out,
    staged, gains_in, whole, normed, gate, hidden, part, parts_in, squares, squares_in,
    send_sem, recv_sem, stage_sem, tok_send, tok_recv, tok_own,
    rs_send, rs_recv, sq_send, sq_recv,
):
    weights, outs = (gate_weight, up_weight, down_weight), (gate_out, up_out, down_out)
    depth, width = gate_weight.shape
    half = depth // 2
    rows, block = tokens.shape
    me_fs, me = lax.axis_index("fs"), lax.axis_index("tp")
    z, x = me_fs // cols, lax.rem(me_fs, cols)
    finals = []

    sides = {
        UP: (z < lines - 1, me_fs + cols),
        DOWN: (z > 0, me_fs - cols),
        RIGHT: (x < cols - 1, me_fs + 1),
        LEFT: (x > 0, me_fs - 1),
    }
    peers = [lax.rem(me + j, tp) for j in range(1, tp)]

    def piece(m, which, shard):
        if m < 2:
            return outs[m].at[pl.ds(pl.multiple_of(shard * depth, 16), depth), :]
        return outs[2].at[pl.ds(pl.multiple_of(shard * depth + which * half, 16), half), :]

    def describe(m, which, shard, side, target):
        ref = piece(m, which, shard)
        return pltpu.make_async_remote_copy(
            src_ref=ref, dst_ref=ref,
            send_sem=send_sem.at[m, which, shard, side],
            recv_sem=recv_sem.at[m, which, shard],
            device_id={"fs": target, "tp": me}, device_id_type=MESH,
        )

    def send(m, which, shard, side, extra=None):
        there, target = sides[side]
        cond = there if extra is None else jnp.logical_and(there, extra)

        @pl.when(cond)
        def _():
            describe(m, which, shard, side, target).start()

        def finish():
            @pl.when(cond)
            def _():
                describe(m, which, shard, side, target).wait_send()

        finals.append(finish)

    def arrive(m, which, shard, cond):
        @pl.when(cond)
        def _():
            describe(m, which, shard, 0, lax.rem(me_fs + 1, fs)).wait_recv()

    barrier = pltpu.get_barrier_semaphore()
    for side in sides:
        there, target = sides[side]

        @pl.when(there)
        def _():
            pl.semaphore_signal(barrier, inc=1, device_id={"fs": target, "tp": me}, device_id_type=MESH)

    for peer in peers:
        pl.semaphore_signal(barrier, inc=1, device_id={"fs": me_fs, "tp": peer}, device_id_type=MESH)

    stages = [pltpu.make_async_copy(weights[m], staged.at[m], stage_sem.at[m]) for m in range(3)]
    for c in stages:
        c.start()
    own_tokens = pltpu.make_async_copy(tokens, whole.at[me], tok_own)
    own_tokens.start()
    gains_in[...] = jnp.transpose(jnp.broadcast_to(pre_gain[0:1, :], (128, depth)))

    def cast(m):
        stages[m].wait()

        @pl.loop(0, depth // 16)
        def _(i):
            here = pl.ds(pl.multiple_of(i * 16, 16), 16)
            v = staged[m, here, :]
            if m < 2:
                v = gains_in[here, 0:1] * v
            outs[m][pl.ds(pl.multiple_of(me_fs * depth + i * 16, 16), 16), :] = v.astype(jnp.bfloat16)

    def token_copy(j):
        return pltpu.make_async_remote_copy(
            src_ref=tokens, dst_ref=whole.at[me], send_sem=tok_send.at[j], recv_sem=tok_recv.at[j],
            device_id={"fs": me_fs, "tp": peers[j]}, device_id_type=MESH,
        )

    def start_own(m):
        for side in (UP, DOWN, RIGHT, LEFT):
            send(m, Q_PART, me_fs, side)

    cast(0)
    pl.semaphore_wait(barrier, tp - 1 + sum(there.astype(jnp.int32) for there, _ in sides.values()))
    start_own(0)
    for j in range(tp - 1):
        token_copy(j).start()
    cast(1)
    cast(2)

    def normalize():
        own_tokens.wait()
        for j in range(tp - 1):
            token_copy(j).wait_recv()
        step = 64

        @pl.loop(0, rows // step)
        def _(i):
            here = pl.ds(pl.multiple_of(i * step, step), step)
            total = jnp.zeros((step, 1), jnp.float32)
            for t in range(tp):
                v = whole[t, here, :].astype(jnp.float32)
                total = total + jnp.sum(v * v, axis=1, keepdims=True)
            scale = lax.rsqrt(total / (tp * block) + EPS)
            for t in range(tp):
                v = whole[t, here, :].astype(jnp.float32)
                normed[here, t * block:(t + 1) * block] = (v * scale).astype(jnp.bfloat16)

    def along_x(m, which, line, cond=None):
        for r in range(cols - 1):
            for side, column in ((RIGHT, x - 1 - r), (LEFT, x + 1 + r)):
                there = jnp.logical_and(column >= 0, column < cols)
                if cond is not None:
                    there = jnp.logical_and(there, cond)
                arrive(m, which, line * cols + column, there)
                if r < cols - 2:
                    send(m, which, line * cols + column, side, there)

    def valid(line):
        return jnp.logical_and(line >= 0, line < lines)

    def along_z(m, which, s, columns):
        for side, line in ((UP, z - 1 - s), (DOWN, z + 1 + s)):
            there = valid(line)
            for column in columns:
                shard = line * cols + column
                arrive(m, which, shard, there)
                if s < lines - 2:
                    send(m, which, shard, side, there)
                if which == Q_PART:
                    send(m, which, shard, RIGHT, there)
                    send(m, which, shard, LEFT, there)

    tile = 256

    def project(m):
        along_x(m, Q_PART, z)
        for s in range(lines - 1):
            for line in (z - 1 - s, z + 1 + s):
                along_x(m, Q_PART, line, valid(line))

        @pl.loop(0, width // tile)
        def _(i):
            here = pl.ds(pl.multiple_of(i * tile, tile), tile)
            product = jnp.dot(normed[...], outs[m][:, here], preferred_element_type=jnp.float32)
            if m == 0:
                gate[:, here] = product
            else:
                g = gate[:, here]
                hidden[:, here] = (g / (1.0 + jnp.exp(-g)) * product).astype(jnp.bfloat16)

    early = max(0, lines - 3)
    for s in range(lines - 1):
        along_z(0, Q_PART, s, [x])
        if s == early:
            start_own(1)
            for side in (RIGHT, LEFT):
                send(2, P_PART, me_fs, side)
    normalize()
    for s in range(lines - 1):
        along_z(1, Q_PART, s, [x])
        if s == 0:
            project(0)
        if s == early:
            start_own(2)
            along_x(2, P_PART, z)
            for column in range(cols):
                for side in (UP, DOWN):
                    send(2, P_PART, z * cols + column, side)

    def share_copy(line, sender, column, which):
        return pltpu.make_async_remote_copy(
            src_ref=part.at[line, column, which], dst_ref=parts_in.at[sender, column, which],
            send_sem=rs_send.at[line, column, which], recv_sem=rs_recv.at[sender, column, which],
            device_id={"fs": me_fs, "tp": line}, device_id_type=MESH,
        )

    def mix(line, column, which):
        here = pl.ds(pl.multiple_of((line * cols + column) * depth + which * half, 16), half)
        product = lax.dot_general(
            hidden[...], outs[2][here, :], (((1,), (1,)), ((), ())), preferred_element_type=jnp.float32
        )
        part[line, column, which] = product.astype(jnp.bfloat16)

        @pl.when(line != me)
        def _():
            share_copy(line, me, column, which).start()

    def mix_both(s, column, which):
        @pl.loop(0, 2)
        def _(i):
            line = z + (1 + s) * (2 * i - 1)

            @pl.when(valid(line))
            def _():
                mix(line, column, which)

    def others(action):
        for j in range(1, cols):
            action(lax.rem(x + j, cols))

    def near(s):
        mix_both(s, x, Q_PART)

        @pl.loop(0, cols)
        def _(c):
            mix_both(s, lax.rem(x + c, cols), P_PART)

    def far(s):
        for line in (z - 1 - s, z + 1 + s):
            along_x(2, Q_PART, line, valid(line))
        others(lambda column: mix_both(s, column, Q_PART))

    for s in range(lines - 1):
        along_z(2, Q_PART, s, [x])
        along_z(2, P_PART, s, range(cols))
        if s == 0:
            project(1)
            mix(z, x, Q_PART)

            @pl.loop(0, cols)
            def _(c):
                mix(z, lax.rem(x + c, cols), P_PART)
        near(s)
        if s == 0:
            along_x(2, Q_PART, z)
            others(lambda column: mix(z, column, Q_PART))
        else:
            far(s - 1)
    far(lines - 2)

    for peer in peers:
        for column in range(cols):
            for which in range(2):
                share_copy(peer, peer, column, which).wait_recv()
    step = 128

    @pl.loop(0, rows // step)
    def _(i):
        here = pl.ds(pl.multiple_of(i * step, step), step)
        square = jnp.zeros((step, 1), jnp.float32)
        for column in range(cols):
            for which in range(2):
                start = column * depth + which * half
                total = part[me, column, which, here, :].astype(jnp.float32)
                for peer in peers:
                    total = total + parts_in[peer, column, which, here, :].astype(jnp.float32)
                gate[here, start:start + half] = total
                square = square + jnp.sum(total * total, axis=1, keepdims=True)
        squares[:, here] = jnp.transpose(jnp.broadcast_to(square, (step, 128)))[0:8, :]

    def square_copy(j):
        return pltpu.make_async_remote_copy(
            src_ref=squares, dst_ref=squares_in.at[j], send_sem=sq_send.at[j], recv_sem=sq_recv.at[j],
            device_id={"fs": me_fs, "tp": peers[j]}, device_id_type=MESH,
        )

    for j in range(tp - 1):
        square_copy(j).start()
    for finish in finals:
        finish()
    for j in range(tp - 1):
        token_copy(j).wait_send()
        for column in range(cols):
            for which in range(2):
                share_copy(peers[j], me, column, which).wait_send()
    for j in range(tp - 1):
        square_copy(j).wait_recv()
    gains = post_gain[0:1, :]

    @pl.loop(0, rows // step)
    def _(i):
        here = pl.ds(pl.multiple_of(i * step, step), step)
        total = squares[:, here]
        for j in range(tp - 1):
            total = total + squares_in[j, :, here]
        total = jnp.broadcast_to(total[0:1, :], (128, step))
        scale = lax.rsqrt(jnp.transpose(total)[:, 0:1] / (tp * block) + EPS)
        result[here, :] = (gate[here, 0:block] * scale * gains).astype(jnp.bfloat16)

    for j in range(tp - 1):
        square_copy(j).wait_send()


def write_out(*refs):
    count = (len(refs) - 1) // 2
    copies = [pltpu.make_async_copy(refs[k], refs[count + k], refs[-1].at[k]) for k in range(count)]
    for c in copies:
        c.start()
    for c in copies:
        c.wait()


def solution(mesh):
    fs, tp = mesh.shape["fs"], mesh.shape["tp"]
    lines, cols = tp, fs // tp

    def shards(tokens, pre_gain, gate_weight, up_weight, down_weight, post_gain):
        depth, width = gate_weight.shape
        rows, block = tokens.shape
        hbm = pl.BlockSpec(memory_space=pltpu.HBM)
        vmem = pl.BlockSpec(memory_space=pltpu.VMEM)
        dma = pltpu.SemaphoreType.DMA
        half = depth // 2
        shapes = [(rows, block)] + [(fs * depth, width)] * 3
        held = pl.pallas_call(
            functools.partial(kernel, fs, tp, lines, cols),
            out_shape=tuple(pltpu.VMEM(s, jnp.bfloat16) for s in shapes),
            in_specs=[hbm, vmem, hbm, hbm, hbm, vmem],
            out_specs=(vmem,) * 4,
            scratch_shapes=[
                pltpu.VMEM((3, depth, width), jnp.float32),
                pltpu.VMEM((depth, 128), jnp.float32),
                pltpu.VMEM((tp, rows, block), jnp.bfloat16),
                pltpu.VMEM((rows, tp * block), jnp.bfloat16),
                pltpu.VMEM((rows, max(width, block)), jnp.float32),
                pltpu.VMEM((rows, width), jnp.bfloat16),
                pltpu.VMEM((tp, cols, 2, rows, half), jnp.bfloat16),
                pltpu.VMEM((tp, cols, 2, rows, half), jnp.bfloat16),
                pltpu.VMEM((8, rows), jnp.float32),
                pltpu.VMEM((tp - 1, 8, rows), jnp.float32),
                dma((3, 2, fs, 4)), dma((3, 2, fs)), dma((3,)),
                dma((tp - 1,)), dma((tp - 1,)), dma,
                dma((tp, cols, 2)), dma((tp, cols, 2)), dma((tp - 1,)), dma((tp - 1,)),
            ],
            compiler_params=pltpu.CompilerParams(collective_id=0, has_side_effects=True, vmem_limit_bytes=42 * 1024 * 1024),
        )(tokens, pre_gain[None, :], gate_weight, up_weight, down_weight, post_gain[None, :])
        return tuple(pl.pallas_call(
            write_out,
            out_shape=tuple(jax.ShapeDtypeStruct(s, jnp.bfloat16) for s in shapes),
            in_specs=[vmem] * 4,
            out_specs=(hbm,) * 4,
            scratch_shapes=[dma((4,))],
            compiler_params=pltpu.CompilerParams(vmem_limit_bytes=1024 * 1024),
        )(*held))

    return jax.shard_map(
        shards,
        mesh=mesh,
        in_specs=(P("fs", "tp"), P("fs"), P("fs", "tp"), P("fs", "tp"), P("fs", "tp"), P("tp")),
        out_specs=(P("fs", "tp"), P(None, "tp"), P(None, "tp"), P(None, "tp")),
        check_vma=False,
    )
```

time: 230 us -> 214 us (0.930)
  local copies, waits for them, and re-layouts: 15.7 us -> 0 us
  Pallas kernels: 208 us -> 214 us
  other arithmetic: 5.45 us -> 0 us
    unnamed x14 -> x0, local copies, waits for them, and re-layouts: 15.7 us -> none
    pallas_call x1 -> x2, Pallas kernels: 208 us -> 214 us  [the longest x1 207 us: shards(): pl.pallas_call(functools.partial(kernel, fs, tp, lines, cols), out_shape=...]
    convert_element_type x2 -> x0, other arithmetic: 5.45 us -> none  [the longest x1 2.96 us: shards(): up_own = (pre_gain[:, None] * up_weight).astype(jnp.bfloat16)]
where the time goes in v2:
time: 214 us
  Pallas kernels  214 us (100%)
    pallas_call x1, Pallas kernels, shards(): pl.pallas_call(functools.partial(kernel, fs, tp, lines, cols), out_shape=...  207 us
    pallas_call x1, Pallas kernels, shards(): pl.pallas_call(write_out, out_shape=tuple((jax.ShapeDtypeStruct(s, jnp.bf...  6.88 us

profile of v2, /device:TPU:0, one launch (start us, length us, event | category | flops | bytes accessed | tf_op | source)
XLA Modules:
  0.0 214.3 jit_solution(405611590772843911)
XLA Ops:
  0.6 206.8 %shard_map.93 = (bf16[512,512]{1,0:T(8,128)(2,1)S(1)}, bf16[2048,1536]{1,0:T(8,128)(2,1)S(1)}, bf16[2048,1536]{1,0:T(8,128)(2,1)S(1)}, bf16[2048,1536]{1,0:T(8,128)(2,1)S(1)}) custom-call(bf16[512,512]{1,0:T(8,128)(2,1)} %tokens.1, f32[1,256]{1,0:T(1,128)} %bitcast.3, f32[256,1536]{1,0:T(8,128)} %gate_weight.1, f32[256,1536]{1,0:T(8,128)} %up_weight.1, ...), custom_call_target="tpu_custom_call" | custom-call | tf_op jit(solution)/shard_map/pallas_call | solution.py:336
  207.4 6.9 %shard_map.94 = (bf16[512,512]{1,0:T(8,128)(2,1)}, bf16[2048,1536]{1,0:T(8,128)(2,1)}, bf16[2048,1536]{1,0:T(8,128)(2,1)}, bf16[2048,1536]{1,0:T(8,128)(2,1)}) custom-call(bf16[512,512]{1,0:T(8,128)(2,1)S(1)} %get-tuple-element.8.refs_0_, bf16[2048,1536]{1,0:T(8,128)(2,1)S(1)} %get-tuple-element.9.refs_1_, bf16[2048,1536]{1,0:T(8,128)(2,1)S(1)} %get-tuple-element.10.refs_2_, ...), custom_call_target="tpu_custom_call" | custom-call | tf_op jit(solution)/shard_map/pallas_call | solution.py:358

commit v3 on v2

--- a/solution.py
+++ b/solution.py
@@ -149,9 +149,9 @@
     def valid(line):
         return jnp.logical_and(line >= 0, line < lines)
 
-    def along_z(m, which, s, columns):
+    def along_z(m, which, s, columns, cond=None):
         for side, line in ((UP, z - 1 - s), (DOWN, z + 1 + s)):
-            there = valid(line)
+            there = valid(line) if cond is None else jnp.logical_and(valid(line), cond)
             for column in columns:
                 shard = line * cols + column
                 arrive(m, which, shard, there)
@@ -189,14 +189,13 @@
     normalize()
     for s in range(lines - 1):
         along_z(1, Q_PART, s, [x])
-        if s == 0:
-            project(0)
         if s == early:
             start_own(2)
             along_x(2, P_PART, z)
             for column in range(cols):
                 for side in (UP, DOWN):
                     send(2, P_PART, z * cols + column, side)
+            project(0)
 
     def share_copy(line, sender, column, which):
         return pltpu.make_async_remote_copy(
@@ -241,23 +240,47 @@
             along_x(2, Q_PART, line, valid(line))
         others(lambda column: mix_both(s, column, Q_PART))
 
-    for s in range(lines - 1):
-        along_z(2, Q_PART, s, [x])
-        along_z(2, P_PART, s, range(cols))
-        if s == 0:
-            project(1)
-            mix(z, x, Q_PART)
-
-            @pl.loop(0, cols)
-            def _(c):
-                mix(z, lax.rem(x + c, cols), P_PART)
-        near(s)
-        if s == 0:
+    inner = jnp.logical_and(z > 0, z < lines - 1)
+
+    def down_step(s, cond=None):
+        along_z(2, Q_PART, s, [x], cond)
+        along_z(2, P_PART, s, range(cols), cond)
+
+    down_step(0)
+    for s in range(1, lines - 2):
+        down_step(s, inner)
+    project(1)
+    mix(z, x, Q_PART)
+
+    @pl.loop(0, cols)
+    def _(c):
+        mix(z, lax.rem(x + c, cols), P_PART)
+
+    if lines > 2:
+        near(0)
+    for s in range(1, lines - 2):
+        down_step(s, jnp.logical_not(inner))
+        if s == 1:
             along_x(2, Q_PART, z)
             others(lambda column: mix(z, column, Q_PART))
-        else:
-            far(s - 1)
-    far(lines - 2)
+        near(s)
+        far(s - 1)
+    last = lines - 2
+    if last > 0:
+        along_z(2, Q_PART, last, [x])
+        mix_both(last, x, Q_PART)
+    else:
+        mix_both(last, x, Q_PART)
+    if last < 2:
+        along_x(2, Q_PART, z)
+        others(lambda column: mix(z, column, Q_PART))
+    if last > 0:
+        far(last - 1)
+    for column in range(cols):
+        if last > 0:
+            along_z(2, P_PART, last, [column])
+        mix_both(last, column, P_PART)
+    far(last)
 
     for peer in peers:
         for column in range(cols):

time: 214 us -> 207 us (0.967)
  Pallas kernels: 214 us -> 207 us
    pallas_call x1, Pallas kernels: 207 us -> 200 us  [shards(): pl.pallas_call(functools.partial(kernel, fs, tp, lines, cols), out_shape=...]
where the time goes in v3:
time: 207 us
  Pallas kernels  207 us (100%)
    pallas_call x1, Pallas kernels, shards(): pl.pallas_call(functools.partial(kernel, fs, tp, lines, cols), out_shape=...  200 us
    pallas_call x1, Pallas kernels, shards(): pl.pallas_call(write_out, out_shape=tuple((jax.ShapeDtypeStruct(s, jnp.bf...  6.88 us

profile of v3, /device:TPU:0, one launch (start us, length us, event | category | flops | bytes accessed | tf_op | source)
XLA Modules:
  0.0 207.2 jit_solution(5137801774249239638)
XLA Ops:
  0.6 199.7 %shard_map.93 = (bf16[512,512]{1,0:T(8,128)(2,1)S(1)}, bf16[2048,1536]{1,0:T(8,128)(2,1)S(1)}, bf16[2048,1536]{1,0:T(8,128)(2,1)S(1)}, bf16[2048,1536]{1,0:T(8,128)(2,1)S(1)}) custom-call(bf16[512,512]{1,0:T(8,128)(2,1)} %tokens.1, f32[1,256]{1,0:T(1,128)} %bitcast.3, f32[256,1536]{1,0:T(8,128)} %gate_weight.1, f32[256,1536]{1,0:T(8,128)} %up_weight.1, ...), custom_call_target="tpu_custom_call" | custom-call | tf_op jit(solution)/shard_map/pallas_call | solution.py:359
  200.3 6.9 %shard_map.94 = (bf16[512,512]{1,0:T(8,128)(2,1)}, bf16[2048,1536]{1,0:T(8,128)(2,1)}, bf16[2048,1536]{1,0:T(8,128)(2,1)}, bf16[2048,1536]{1,0:T(8,128)(2,1)}) custom-call(bf16[512,512]{1,0:T(8,128)(2,1)S(1)} %get-tuple-element.8.refs_0_, bf16[2048,1536]{1,0:T(8,128)(2,1)S(1)} %get-tuple-element.9.refs_1_, bf16[2048,1536]{1,0:T(8,128)(2,1)S(1)} %get-tuple-element.10.refs_2_, ...), custom_call_target="tpu_custom_call" | custom-call | tf_op jit(solution)/shard_map/pallas_call | solution.py:381

commit v4 on v3

--- a/solution.py
+++ b/solution.py
@@ -11,6 +11,7 @@
 MESH = pl.DeviceIdType.MESH
 P_PART, Q_PART = 0, 1
 UP, DOWN, RIGHT, LEFT = 0, 1, 2, 3
+CHUNKS = 4
 
 
 def kernel(
@@ -106,8 +107,8 @@
             device_id={"fs": me_fs, "tp": peers[j]}, device_id_type=MESH,
         )
 
-    def start_own(m):
-        for side in (UP, DOWN, RIGHT, LEFT):
+    def start_own(m, which_sides=(UP, DOWN, RIGHT, LEFT)):
+        for side in which_sides:
             send(m, Q_PART, me_fs, side)
 
     cast(0)
@@ -190,12 +191,13 @@
     for s in range(lines - 1):
         along_z(1, Q_PART, s, [x])
         if s == early:
-            start_own(2)
+            start_own(2, (UP, DOWN))
             along_x(2, P_PART, z)
             for column in range(cols):
                 for side in (UP, DOWN):
                     send(2, P_PART, z * cols + column, side)
             project(0)
+    start_own(2, (RIGHT, LEFT))
 
     def share_copy(line, sender, column, which):
         return pltpu.make_async_remote_copy(
@@ -337,7 +339,12 @@
 
 def write_out(*refs):
     count = (len(refs) - 1) // 2
-    copies = [pltpu.make_async_copy(refs[k], refs[count + k], refs[-1].at[k]) for k in range(count)]
+    copies = []
+    for k in range(count):
+        size = refs[k].shape[0] // CHUNKS
+        for c in range(CHUNKS):
+            here = pl.ds(c * size, size)
+            copies.append(pltpu.make_async_copy(refs[k].at[here, :], refs[count + k].at[here, :], refs[-1].at[k, c]))
     for c in copies:
         c.start()
     for c in copies:
@@ -383,7 +390,7 @@
             out_shape=tuple(jax.ShapeDtypeStruct(s, jnp.bfloat16) for s in shapes),
             in_specs=[vmem] * 4,
             out_specs=(hbm,) * 4,
-            scratch_shapes=[dma((4,))],
+            scratch_shapes=[dma((4, CHUNKS))],
             compiler_params=pltpu.CompilerParams(vmem_limit_bytes=1024 * 1024),
         )(*held))
 

time: 207 us -> 206 us (level)
  no operation moved by 1% of the time
where the time goes in v4:
time: 206 us
  Pallas kernels  205 us (100%)
    pallas_call x1, Pallas kernels, shards(): pl.pallas_call(functools.partial(kernel, fs, tp, lines, cols), out_shape=...  199 us
    pallas_call x1, Pallas kernels, shards(): pl.pallas_call(write_out, out_shape=tuple((jax.ShapeDtypeStruct(s, jnp.bf...  6.79 us

profile of v4, /device:TPU:0, one launch (start us, length us, event | category | flops | bytes accessed | tf_op | source)
XLA Modules:
  0.0 206.1 jit_solution(8893048576351589892)
XLA Ops:
  0.6 198.7 %shard_map.93 = (bf16[512,512]{1,0:T(8,128)(2,1)S(1)}, bf16[2048,1536]{1,0:T(8,128)(2,1)S(1)}, bf16[2048,1536]{1,0:T(8,128)(2,1)S(1)}, bf16[2048,1536]{1,0:T(8,128)(2,1)S(1)}) custom-call(bf16[512,512]{1,0:T(8,128)(2,1)} %tokens.1, f32[1,256]{1,0:T(1,128)} %bitcast.3, f32[256,1536]{1,0:T(8,128)} %gate_weight.1, f32[256,1536]{1,0:T(8,128)} %up_weight.1, ...), custom_call_target="tpu_custom_call" | custom-call | tf_op jit(solution)/shard_map/pallas_call | solution.py:366
  199.3 6.8 %shard_map.94 = (bf16[512,512]{1,0:T(8,128)(2,1)}, bf16[2048,1536]{1,0:T(8,128)(2,1)}, bf16[2048,1536]{1,0:T(8,128)(2,1)}, bf16[2048,1536]{1,0:T(8,128)(2,1)}) custom-call(bf16[512,512]{1,0:T(8,128)(2,1)S(1)} %get-tuple-element.8.refs_0_, bf16[2048,1536]{1,0:T(8,128)(2,1)S(1)} %get-tuple-element.9.refs_1_, bf16[2048,1536]{1,0:T(8,128)(2,1)S(1)} %get-tuple-element.10.refs_2_, ...), custom_call_target="tpu_custom_call" | custom-call | tf_op jit(solution)/shard_map/pallas_call | solution.py:388

commit v5 on v4

--- a/solution.py
+++ b/solution.py
@@ -16,9 +16,9 @@
 
 def kernel(
     fs, tp, lines, cols,
-    tokens, pre_gain, gate_weight, up_weight, down_weight, post_gain,
-    result, gate_out, up_out, down_out,
-    staged, gains_in, whole, normed, gate, hidden, part, parts_in, squares, squares_in,
+    tokens, pre_gain, gate_weight, up_weight, down_weight,
+    gate, squares, squares_in, gate_out, up_out, down_out,
+    staged, gains_in, whole, normed, hidden, part, parts_in,
     send_sem, recv_sem, stage_sem, tok_send, tok_recv, tok_own,
     rs_send, rs_recv, sq_send, sq_recv,
 ):
@@ -321,34 +321,41 @@
                 share_copy(peers[j], me, column, which).wait_send()
     for j in range(tp - 1):
         square_copy(j).wait_recv()
+    for j in range(tp - 1):
+        square_copy(j).wait_send()
+
+
+def write_out(
+    width, share, squares, squares_in, gate_held, up_held, down_held, post_gain,
+    result_out, gate_out, up_out, down_out, result, sems, last,
+):
+    copies = []
+    for k, (ref, out) in enumerate(((gate_held, gate_out), (up_held, up_out), (down_held, down_out))):
+        size = ref.shape[0] // CHUNKS
+        for c in range(CHUNKS):
+            here = pl.ds(c * size, size)
+            copies.append(pltpu.make_async_copy(ref.at[here, :], out.at[here, :], sems.at[k, c]))
+    for c in copies:
+        c.start()
+    rows, block = result.shape
     gains = post_gain[0:1, :]
+    step = 128
 
     @pl.loop(0, rows // step)
     def _(i):
         here = pl.ds(pl.multiple_of(i * step, step), step)
         total = squares[:, here]
-        for j in range(tp - 1):
+        for j in range(squares_in.shape[0]):
             total = total + squares_in[j, :, here]
         total = jnp.broadcast_to(total[0:1, :], (128, step))
-        scale = lax.rsqrt(jnp.transpose(total)[:, 0:1] / (tp * block) + EPS)
-        result[here, :] = (gate[here, 0:block] * scale * gains).astype(jnp.bfloat16)
-
-    for j in range(tp - 1):
-        square_copy(j).wait_send()
-
-
-def write_out(*refs):
-    count = (len(refs) - 1) // 2
-    copies = []
-    for k in range(count):
-        size = refs[k].shape[0] // CHUNKS
-        for c in range(CHUNKS):
-            here = pl.ds(c * size, size)
-            copies.append(pltpu.make_async_copy(refs[k].at[here, :], refs[count + k].at[here, :], refs[-1].at[k, c]))
-    for c in copies:
-        c.start()
+        scale = lax.rsqrt(jnp.transpose(total)[:, 0:1] / width + EPS)
+        result[here, :] = (share[here, 0:block] * scale * gains).astype(jnp.bfloat16)
+
+    final = pltpu.make_async_copy(result, result_out, last)
+    final.start()
     for c in copies:
         c.wait()
+    final.wait()
 
 
 def solution(mesh):
@@ -365,34 +372,35 @@
         shapes = [(rows, block)] + [(fs * depth, width)] * 3
         held = pl.pallas_call(
             functools.partial(kernel, fs, tp, lines, cols),
-            out_shape=tuple(pltpu.VMEM(s, jnp.bfloat16) for s in shapes),
-            in_specs=[hbm, vmem, hbm, hbm, hbm, vmem],
-            out_specs=(vmem,) * 4,
+            out_shape=(
+                pltpu.VMEM((rows, max(width, block)), jnp.float32),
+                pltpu.VMEM((8, rows), jnp.float32),
+                pltpu.VMEM((tp - 1, 8, rows), jnp.float32),
+            ) + tuple(pltpu.VMEM(s, jnp.bfloat16) for s in shapes[1:]),
+            in_specs=[hbm, vmem, hbm, hbm, hbm],
+            out_specs=(vmem,) * 6,
             scratch_shapes=[
                 pltpu.VMEM((3, depth, width), jnp.float32),
                 pltpu.VMEM((depth, 128), jnp.float32),
                 pltpu.VMEM((tp, rows, block), jnp.bfloat16),
                 pltpu.VMEM((rows, tp * block), jnp.bfloat16),
-                pltpu.VMEM((rows, max(width, block)), jnp.float32),
                 pltpu.VMEM((rows, width), jnp.bfloat16),
                 pltpu.VMEM((tp, cols, 2, rows, half), jnp.bfloat16),
                 pltpu.VMEM((tp, cols, 2, rows, half), jnp.bfloat16),
-                pltpu.VMEM((8, rows), jnp.float32),
-                pltpu.VMEM((tp - 1, 8, rows), jnp.float32),
                 dma((3, 2, fs, 4)), dma((3, 2, fs)), dma((3,)),
                 dma((tp - 1,)), dma((tp - 1,)), dma,
                 dma((tp, cols, 2)), dma((tp, cols, 2)), dma((tp - 1,)), dma((tp - 1,)),
             ],
-            compiler_params=pltpu.CompilerParams(collective_id=0, has_side_effects=True, vmem_limit_bytes=42 * 1024 * 1024),
-        )(tokens, pre_gain[None, :], gate_weight, up_weight, down_weight, post_gain[None, :])
+            compiler_params=pltpu.CompilerParams(collective_id=0, has_side_effects=True, vmem_limit_bytes=38 * 1024 * 1024),
+        )(tokens, pre_gain[None, :], gate_weight, up_weight, down_weight)
         return tuple(pl.pallas_call(
-            write_out,
+            functools.partial(write_out, tp * block),
             out_shape=tuple(jax.ShapeDtypeStruct(s, jnp.bfloat16) for s in shapes),
-            in_specs=[vmem] * 4,
+            in_specs=[vmem] * 7,
             out_specs=(hbm,) * 4,
-            scratch_shapes=[dma((4, CHUNKS))],
-            compiler_params=pltpu.CompilerParams(vmem_limit_bytes=1024 * 1024),
-        )(*held))
+            scratch_shapes=[pltpu.VMEM((rows, block), jnp.bfloat16), dma((3, CHUNKS)), dma],
+            compiler_params=pltpu.CompilerParams(vmem_limit_bytes=2 * 1024 * 1024),
+        )(*held, post_gain[None, :]))
 
     return jax.shard_map(
         shards,

time: 206 us -> 206 us (level)
  no operation moved by 1% of the time
where the time goes in v5:
time: 206 us
  Pallas kernels  205 us (100%)
    pallas_call x1, Pallas kernels, shards(): pl.pallas_call(functools.partial(kernel, fs, tp, lines, cols), out_shape=...  198 us
    pallas_call x1, Pallas kernels, shards(): pl.pallas_call(functools.partial(write_out, tp * block), out_shape=tuple(...  6.71 us

profile of v5, /device:TPU:0, one launch (start us, length us, event | category | flops | bytes accessed | tf_op | source)
XLA Modules:
  0.0 206.0 jit_solution(15746758589593282276)
XLA Ops:
  0.6 197.9 %shard_map.93 = (f32[512,1536]{1,0:T(8,128)S(1)}, f32[8,512]{1,0:T(8,128)S(1)}, f32[3,8,512]{2,1,0:T(8,128)S(1)}, bf16[2048,1536]{1,0:T(8,128)(2,1)S(1)}, bf16[2...) custom-call(bf16[512,512]{1,0:T(8,128)(2,1)} %tokens.1, f32[1,256]{1,0:T(1,128)} %bitcast.3, ...), custom_call_target="tpu_custom_call" | custom-call | tf_op jit(solution)/shard_map/pallas_call | solution.py:373
  198.6 0.0 copy-start
  198.6 0.7 copy-done
  199.3 6.7 %shard_map.94 = (bf16[512,512]{1,0:T(8,128)(2,1)}, bf16[2048,1536]{1,0:T(8,128)(2,1)}, bf16[2048,1536]{1,0:T(8,128)(2,1)}, bf16[2048,1536]{1,0:T(8,128)(2,1)}) custom-call(f32[512,1536]{1,0:T(8,128)S(1)} %get-tuple-element.10.share, f32[8,512]{1,0:T(8,128)S(1)} %get-tuple-element.11.squares, f32[3,8,512]{2,1,0:T(8,128)S(1)} %get-tuple-element.12.squares_in, ...), custom_call_target="tpu_custom_call" | custom-call | tf_op jit(solution)/shard_map/pallas_call | solution.py:396
Async XLA Ops:
  198.6 0.7 copy-start
